TPU v7x, 32 devices: a whole 2x2x4 slice. The times are simulated.
32 devices in a mesh: ep: 8 (over z, y), tp: 4 (over x, core).
Axes of the slice: x: 2, y: 2, z: 4, core: 2. Of those that a mesh axis runs over, the one named last changes fastest.
Arguments:
- query_rows: bfloat16 [8192, 1024], P('ep', 'tp'), may hold values from -140 to 140
- key_rows: bfloat16 [8192, 256], P('ep', 'tp'), may hold values from -4.5 to 4.5
- value_rows: bfloat16 [8192, 256], P('ep', 'tp'), may hold values from -6 to 6
- sink_logit: float32 [16], P('tp'), may hold values from 1 to 6
- out_weight: bfloat16 [1024, 2048], P('tp'), may hold values from -0.1875 to 0.1875
- routed_rows: bfloat16 [4096, 2048], P(('ep', 'tp')), may hold values from -6 to 6
- norm_gain: float32 [2048], replicated, may hold values from 0.1 to 1.9
- routing: int32 [4096, 2], P(('ep', 'tp')), may hold values from 0 to 7, all different within a row; in each aligned block of 128 rows (0 to 127, 128 to 255, ...) at most 36 rows name the same one
- route_weight: float32 [4096, 2], P(('ep', 'tp')), may hold values from 0.2 to 1
- gate_weight: bfloat16 [8, 2048, 7168], P('ep', None, 'tp'), may hold values from -0.125 to 0.125
- up_weight: bfloat16 [8, 2048, 7168], P('ep', None, 'tp'), may hold values from -0.125 to 0.125
- down_weight: bfloat16 [8, 7168, 2048], P('ep', 'tp'), may hold values from -0.0625 to 0.0625
Outputs:
- mixed_rows: bfloat16 [8192, 2048], P(('ep', 'tp'))
- expert_mix: bfloat16 [4096, 2048], P(('ep', 'tp'))
Inputs may be any that keep to these rules, and one draw needn't show every extreme that they name: `routing`: each token names 2 different experts. Within the 128 rows of one device no expert is named by more than 36 rows, and in every draw some device's rows name some expert exactly 36 times.
All inputs are finite; a program needn't handle non-finite values.
Results may differ from a plain program's by a relative error of at most 0.012.
Values may be sent and summed in bfloat16 or wider, within the bound.
A program may use at most 128 MiB of HBM per device.

v0:
```python
import jax
import jax.numpy as jnp
from jax import lax
from jax.sharding import PartitionSpec as P

HEAD_DIM = 64
WINDOW = 128


EPS = 1e-06


def padded_2(value, sides, width):
    for axis, dim in sides:
        peers, length = (lax.axis_size(axis), value.shape[dim])
        up = [(i, (i + 1) % peers) for i in range(peers - 1)]
        down = [(j, i) for i, j in up]
        last = lax.slice_in_dim(value, length - width, length, axis=dim)
        leading = lax.slice_in_dim(value, 0, width, axis=dim)
        before = lax.ppermute(last, axis, up)
        after = lax.ppermute(leading, axis, down)
        value = jnp.concatenate([before, value, after], axis=dim)
    return value


def expert_hidden(arrived, gate_weight, up_weight):
    gate_pre = jnp.einsum(
        "scd,df->scf", arrived, gate_weight[0], preferred_element_type=jnp.float32
    )
    up_pre = jnp.einsum("scd,df->scf", arrived, up_weight[0], preferred_element_type=jnp.float32)
    return (jax.nn.silu(gate_pre) * up_pre).astype(jnp.bfloat16)


def window_attention(query_rows, key_rows, value_rows, sink_logit):
    row_count = query_rows.shape[0]
    kv_here = key_rows.shape[1] // HEAD_DIM
    group_size = query_rows.shape[1] // (kv_here * HEAD_DIM)
    block_rows = min(512, row_count)
    joined = jnp.concatenate([key_rows, value_rows], axis=1)
    padded = padded_2(joined, (("ep", 0),), WINDOW)
    seq_total = row_count * lax.axis_size("ep")
    offset = lax.axis_index("ep") * row_count
    sink_col = sink_logit.reshape(kv_here, group_size)[:, :, None]
    score_scale = HEAD_DIM ** (-0.5)

    def one_block(block_index):
        first_row = block_index * block_rows
        query_block = lax.dynamic_slice_in_dim(query_rows, first_row, block_rows, 0).reshape(
            block_rows, kv_here, group_size, HEAD_DIM
        )
        key_span = lax.dynamic_slice_in_dim(padded, first_row, block_rows + 2 * WINDOW, 0)
        key_block = key_span[:, : kv_here * HEAD_DIM].reshape(-1, kv_here, HEAD_DIM)
        value_block = key_span[:, kv_here * HEAD_DIM :].reshape(-1, kv_here, HEAD_DIM)
        scores = (
            jnp.einsum("qkgd,skd->kgqs", query_block, key_block, preferred_element_type=jnp.float32)
            * score_scale
        )
        query_pos = first_row + jnp.arange(block_rows, dtype=jnp.int32)
        key_pos = first_row - WINDOW + jnp.arange(block_rows + 2 * WINDOW, dtype=jnp.int32)
        global_pos = offset + key_pos
        inside = (
            (jnp.abs(key_pos[None, :] - query_pos[:, None]) <= WINDOW)
            & (global_pos >= 0)[None, :]
            & (global_pos < seq_total)[None, :]
        )
        scores = jnp.where(inside, scores, -jnp.inf)
        row_peak = jnp.maximum(jnp.max(scores, axis=-1), sink_col)
        weights = jnp.exp(scores - row_peak[..., None])
        total_weight = jnp.sum(weights, axis=-1) + jnp.exp(sink_col - row_peak)
        attended = jnp.einsum(
            "kgqs,skd->qkgd",
            weights.astype(jnp.bfloat16),
            value_block,
            preferred_element_type=jnp.float32,
        )
        attended = attended / jnp.transpose(total_weight, (2, 0, 1))[..., None]
        return attended.reshape(block_rows, -1).astype(jnp.bfloat16)

    pieces = lax.map(one_block, jnp.arange(row_count // block_rows, dtype=jnp.int32))
    return pieces.reshape(row_count, -1)


def body(
    query_rows,
    key_rows,
    value_rows,
    sink_logit,
    out_weight,
    routed_rows,
    norm_gain,
    routing,
    route_weight,
    gate_weight,
    up_weight,
    down_weight,
):
    attended = window_attention(query_rows, key_rows, value_rows, sink_logit)
    projected = lax.psum_scatter(
        jnp.dot(attended, out_weight, preferred_element_type=jnp.float32).astype(jnp.bfloat16),
        "tp",
        scatter_dimension=0,
        tiled=True,
    )
    token_count, model_width = routed_rows.shape
    top_count = routing.shape[1]
    experts = lax.axis_size("ep")
    capacity = token_count * top_count * 9 // (8 * experts)
    values = routed_rows.astype(jnp.float32)
    normed = (
        values * lax.rsqrt(jnp.mean(values * values, axis=-1, keepdims=True) + EPS) * norm_gain
    ).astype(jnp.bfloat16)
    chosen = routing.reshape(-1)
    onehot = (chosen[:, None] == jnp.arange(experts, dtype=jnp.int32)[None, :]).astype(jnp.int32)
    before = jnp.cumsum(onehot, axis=0) - onehot
    slot_index = jnp.sum(before * onehot, axis=1)
    target = chosen * capacity + slot_index
    outgoing = (
        jnp.zeros((experts * capacity, model_width), jnp.bfloat16)
        .at[target]
        .set(jnp.repeat(normed, top_count, axis=0))
    )
    outgoing = outgoing.reshape(experts, capacity, model_width)
    hidden = expert_hidden(
        lax.all_gather(
            lax.all_to_all(outgoing, "ep", split_axis=0, concat_axis=0, tiled=True),
            "tp",
            axis=0,
            tiled=True,
        ),
        gate_weight,
        up_weight,
    )
    rounded = jnp.einsum(
        "scf,fd->scd", hidden, down_weight[0], preferred_element_type=jnp.float32
    ).astype(jnp.bfloat16)
    summed = lax.psum_scatter(
        lax.optimization_barrier(rounded).astype(jnp.float32).astype(jnp.bfloat16),
        "tp",
        scatter_dimension=0,
        tiled=True,
    ).astype(jnp.float32)
    results = lax.all_to_all(
        summed.astype(jnp.bfloat16), "ep", split_axis=0, concat_axis=0, tiled=True
    ).astype(summed.dtype)
    slot_results = results.reshape(experts * capacity, model_width)
    picked = slot_results[target] * route_weight.reshape(-1)[:, None]
    expert_mix = jnp.sum(picked.reshape(token_count, top_count, model_width), axis=1).astype(
        jnp.bfloat16
    )
    return (projected, expert_mix)


def solution(mesh):
    in_specs = (
        P("ep", "tp"),
        P("ep", "tp"),
        P("ep", "tp"),
        P("tp"),
        P("tp", None),
        P(("ep", "tp"), None),
        P(),
        P(("ep", "tp"), None),
        P(("ep", "tp"), None),
        P("ep", None, "tp"),
        P("ep", None, "tp"),
        P("ep", "tp", None),
    )
    out_specs = (P(("ep", "tp"), None), P(("ep", "tp"), None))
    return jax.shard_map(body, mesh=mesh, in_specs=in_specs, out_specs=out_specs, check_vma=False)
```

profile of v0, /device:TPU:13, one launch (start us, length us, event | category | flops | bytes accessed | tf_op | source)
XLA Modules:
  0.0 252.2 jit_solution(6978425806556693117)
XLA Ops:
  7.2 0.0 copy-start
  7.2 0.0 all-gather.2.cloned.1.call-start
  7.2 0.9 copy.28
  8.1 0.1 eq.29
  8.2 0.1 eq.25
  8.4 0.7 broadcast_multiply_fusion
  9.1 0.6 reduce-window.6
  9.6 0.2 slice_reduce_fusion
  9.9 0.1 copy.27
  10.0 0.1 mul.81
  10.1 1.2 fusion.47
  11.4 1.2 fusion.49
  12.6 0.6 broadcast_in_dim.38
  13.3 1.2 reshape.293
  14.5 0.1 fusion.53
  14.6 3.1 %scatter_custom_fusion = bf16[288,2048]{1,0:T(8,128)(2,1)S(1)} fusion(s32[256]{0:T(256)S(1)} %bitcast.135, bf16[256,2048]{1,0:T(8,128)(2,1)} %reshape.293, bf16[]{:T(256)} %constant.85.clone.1), kind=kCustom, calls=%fused_computation.52 | custom fusion | bytes 1180160 | tf_op jit(solution)/shard_map/scatter | solution.py:120
  17.7 0.3 reshape.276
  18.0 33.9 %all_to_all.10 = bf16[8,36,2048]{2,1,0:T(8,128)(2,1)S(1)} all-to-all(bf16[8,36,2048]{2,1,0:T(8,128)(2,1)S(1)} %reshape.276), channel_id=1, replica_groups=mesh['ep'=8,'tp'=4] {'ep'}, dimensions={0} | all-to-all | bytes 2359296 | tf_op jit(solution)/shard_map/all_to_all | solution.py:125
  51.9 1.7 copy.30
  53.5 0.0 all-gather.2.cloned.1.call-update
  53.6 0.0 reduce-scatter.5.cloned.1.call-start
  53.6 40.0 %all-gather.2.cloned.1.call-done = bf16[32,36,2048]{2,0,1:T(8,128)(2,1)} async-done(((bf16[8,36,2048]{2,0,1:T(8,128)(2,1)}), bf16[32,36,2048]{2,0,1:T(8,128)(2,1)}) %all-gather.2.cloned.1.call-update) | async-done | bytes 4718608 | tf_op jit(solution)/shard_map/all_gather | solution.py:124
  93.6 19.5 %fusion.28 = f32[32,36,1792]{2,1,0:T(8,128)} fusion(bf16[1,2048,1792]{2,1,0:T(8,128)(2,1)} %param.24, bf16[32,36,2048]{2,0,1:T(8,128)(2,1)} %all-gather.2.cloned.1.call-done), kind=kOutput, calls=%fused_computation.37 | convolution fusion | flops 8455716864 | bytes 20316160 | tf_op jit(solution)/shard_map/scd,df->scf/dot_general | solution.py:30
  113.1 33.8 %fusion.40 = bf16[32,36,2048]{2,1,0:T(8,128)(2,1)} fusion(bf16[1,1792,2048]{2,1,0:T(8,128)(2,1)} %param.25, f32[32,36,1792]{2,1,0:T(8,128)} %fusion.28, bf16[1,2048,1792]{2,1,0:T(8,128)(2,1)} %param.23, bf16[32,36,2048]{2,0,1:T(8,128)(2,1)} %all-gather.2.cloned.1.call-done), kind=kOutput, calls=%fused_computation.44 | convolution fusion | flops 16926179328 | bytes 32374784 | tf_op jit(solution)/shard_map/scf,fd->scd/dot_general | solution.py:133
  146.9 0.0 reduce-scatter.5.cloned.1.call-update
  146.9 0.0 reduce-scatter.3.cloned.1.call-start
  147.0 3.2 %collective-permute-start = (bf16[128,128]{0,1:T(8,128)(2,1)S(1)}, bf16[128,128]{0,1:T(8,128)(2,1)S(1)}, u32[]{:S(2)}, u32[]{:S(2)}) collective-permute-start(bf16[128,128]{0,1:T(8,128)(2,1)S(1)} %get-tuple-element.131), channel_id=1, source_target_pairs={{0,4},{4,8},{8,12},{12,16},{16,20},{20,24},{24,28},{1,5},{5,9},{9,... | collective-permute-start | bytes 98312 | tf_op jit(solution)/shard_map/ppermute | solution.py:20
  150.3 2.2 collective-permute-start.1
  152.5 0.0 collective-permute-done
  152.5 3.3 %collective-permute-done.1 = bf16[128,128]{0,1:T(8,128)(2,1)S(1)} collective-permute-done((bf16[128,128]{0,1:T(8,128)(2,1)S(1)}, bf16[128,128]{0,1:T(8,128)(2,1)S(1)}, u32[]{:S(2)}, u32[]{:S(2)}) %collective-permute-start.1) | collective-permute-done | bytes 32800 | tf_op jit(solution)/shard_map/ppermute | solution.py:21
  155.9 25.0 %while.12 = (s32[]{:T(128)}, bf16[2,512,256]{2,1,0:T(8,128)(2,1)S(1)}, s32[2]{0:T(128)S(1)}, bf16[1280,128]{0,1:T(8,128)(2,1)S(1)}, s32[]{:T(128)}, /*index=5*/b...) while((s32[]{:T(128)}, ...), condition=%wide.region_3.4_spmd, body=%wide.region_0.3_spmd.sunk | while | flops 422191360 | bytes 48526672 | solution.py:79
  156.1 0.7 dynamic_slice.23
  157.5 0.8 fusion.69
  158.3 0.1 copy.47
  158.5 1.2 fusion.70
  159.7 0.0 copy-start.1
  159.7 0.1 broadcast_maximum_fusion.2
  159.8 2.6 %copy-done.1 = f32[768,512,4]{1,0,2:T(8,128)} copy-done((f32[768,512,4]{1,0,2:T(8,128)}, f32[768,512,4]{1,0,2:T(8,128)S(1)}, u32[]{:S(2)}) %copy-start.1) | copy-done | bytes 6291480 | tf_op jit(solution)/shard_map/while
  162.4 1.4 fusion.71
  163.7 0.1 fusion.72
  163.8 4.5 %fusion.73 = bf16[512,1,4,64]{0,3,2,1:T(8,128)(2,1)S(1)} fusion(f32[768,512,4]{1,0,2:T(8,128)} %copy-done.1, f32[4,512]{1,0:T(4,128)S(1)} %broadcast_maximum_fusion.2, pred[512,768]{0,1:T(8,128)(4,1)S(1)} %fusion.69, f32[512,4]{0,1:T(4,128)S(1)} %fusion.72, bf16[1280,128]{0,1:T(8,128)(2,1)S(1)} %get-tuple-element.215, s32[]{:T(128)S(6)} %select_n.57, ...), kind=kOutput, calls=%fused_computation.15.clone.1 | convolution fusion | flops 207880192 | bytes 7061512 | tf_op jit(solution)/shard_map/while/body/eval_jaxpr/kgqs,skd->qkgd/dot_general | solution.py:70
  168.3 0.1 copy.48
  168.5 0.7 dynamic_slice.23
  169.9 0.8 fusion.69
  170.7 0.1 copy.47
  170.9 1.2 fusion.70
  172.1 0.1 broadcast_maximum_fusion.2
  172.2 2.6 %copy-done.1 = f32[768,512,4]{1,0,2:T(8,128)} copy-done((f32[768,512,4]{1,0,2:T(8,128)}, f32[768,512,4]{1,0,2:T(8,128)S(1)}, u32[]{:S(2)}) %copy-start.1) | copy-done | bytes 6291480 | tf_op jit(solution)/shard_map/while
  174.7 1.4 fusion.71
  176.1 0.1 fusion.72
  176.2 4.6 %fusion.73 = bf16[512,1,4,64]{0,3,2,1:T(8,128)(2,1)S(1)} fusion(f32[768,512,4]{1,0,2:T(8,128)} %copy-done.1, f32[4,512]{1,0:T(4,128)S(1)} %broadcast_maximum_fusion.2, pred[512,768]{0,1:T(8,128)(4,1)S(1)} %fusion.69, f32[512,4]{0,1:T(4,128)S(1)} %fusion.72, bf16[1280,128]{0,1:T(8,128)(2,1)S(1)} %get-tuple-element.215, s32[]{:T(128)S(6)} %select_n.57, ...), kind=kOutput, calls=%fused_computation.15.clone.1 | convolution fusion | flops 207880192 | bytes 7061512 | tf_op jit(solution)/shard_map/while/body/eval_jaxpr/kgqs,skd->qkgd/dot_general | solution.py:70
  180.8 0.1 copy.48
  181.0 0.0 copy-start.6
  181.0 3.2 %convolution_convert_fusion = bf16[1024,2048]{1,0:T(8,128)(2,1)} fusion(bf16[1024,256]{1,0:T(8,128)(2,1)S(1)} %bitcast.131, bf16[256,2048]{1,0:T(8,128)(2,1)S(1)} %copy-done), kind=kOutput, calls=%fused_computation.45 | convolution fusion | flops 1075838976 | bytes 5767168 | tf_op jit(solution)/shard_map/dot_general | solution.py:99
  184.2 0.0 reduce-scatter.3.cloned.1.call-update
  184.2 13.7 %reduce-scatter.5.cloned.1.call-done = bf16[8,36,2048]{2,1,0:T(8,128)(2,1)} async-done(((bf16[32,36,2048]{2,1,0:T(8,128)(2,1)}), bf16[8,36,2048]{2,1,0:T(8,128)(2,1)}) %reduce-scatter.5.cloned.1.call-update) | async-done | bytes 1179664 | tf_op jit(solution)/shard_map/reduce_scatter | solution.py:136
  197.8 5.5 %all-to-all-start.1 = ((bf16[8,36,2048]{2,1,0:T(8,128)(2,1)}), bf16[8,36,2048]{2,1,0:T(8,128)(2,1)}, u32[]{:S(2)}, u32[]{:S(2)}) async-start(bf16[8,36,2048]{2,1,0:T(8,128)(2,1)} %reduce-scatter.5.cloned.1.call-done), calls=%async_computation.3 | async-start | bytes 2621440 | tf_op jit(solution)/shard_map/all_to_all | solution.py:142
  203.3 0.1 copy.33
  203.4 28.7 %all-to-all-done.1 = bf16[8,36,2048]{2,1,0:T(8,128)(2,1)} async-done(((bf16[8,36,2048]{2,1,0:T(8,128)(2,1)}), bf16[8,36,2048]{2,1,0:T(8,128)(2,1)}, u32[]{:S(2)}, u32[]{:S(2)}) %all-to-all-start.1) | async-done | bytes 1179680 | tf_op jit(solution)/shard_map/all_to_all | solution.py:142
  232.2 1.4 reshape.280
  233.6 2.7 %gather_fusion = f32[256,2048]{1,0:T(8,128)} fusion(f32[288,2048]{1,0:T(8,128)S(1)} %reshape.280, s32[1024]{0:T(1024)S(1)} %pad_clamp_fusion), kind=kCustom, calls=%fused_computation | custom fusion | bytes 4195328 | tf_op jit(solution)/shard_map/gather | solution.py:146
  236.3 2.5 gather.6
  238.8 3.9 %multiply_reduce_fusion = bf16[128,2048]{1,0:T(8,128)(2,1)} fusion(f32[128,2,2048]{2,1,0:T(2,128)S(1)} %gather.6, f32[128,2]{1,0:T(8,128)S(1)} %copy.33), kind=kLoop, calls=%fused_computation.46 | loop fusion | flops 786432 | bytes 2622464 | tf_op jit(solution)/shard_map/reduce_sum | solution.py:147
  242.7 2.9 %reduce-scatter.3.cloned.1.call-done = bf16[256,2048]{1,0:T(8,128)(2,1)} async-done(((bf16[1024,2048]{1,0:T(8,128)(2,1)}), bf16[256,2048]{1,0:T(8,128)(2,1)}) %reduce-scatter.3.cloned.1.call-update) | async-done | bytes 1048592 | tf_op jit(solution)/shard_map/reduce_scatter | solution.py:98
  (33 shorter events, 0.3 us)
Async XLA Ops:
  7.2 173.8 %copy-start = (bf16[256,2048]{1,0:T(8,128)(2,1)S(1)}, bf16[256,2048]{1,0:T(8,128)(2,1)}, u32[]{:S(2)}) copy-start(bf16[256,2048]{1,0:T(8,128)(2,1)} %param.18) | copy-start | bytes 3145732
  7.2 86.4 %all-gather.2.cloned.1.call-start = ((), (), s32[]{:S(2)}) async-start(), calls=%async_computation.5 | async-start | bytes 5898240 | tf_op jit(solution)/shard_map/all_gather | solution.py:124
  53.6 144.3 %reduce-scatter.5.cloned.1.call-start = ((), (), s32[]{:S(2)}) async-start(), calls=%async_computation.6 | async-start | bytes 6553600 | tf_op jit(solution)/shard_map/reduce_scatter | solution.py:136
  113.0 33.9 %copy-start.3 = (bf16[1024,64]{0,1:T(8,128)(2,1)S(1)}, bf16[1024,64]{0,1:T(8,128)(2,1)}, u32[]{:S(2)}) copy-start(bf16[1024,64]{0,1:T(8,128)(2,1)} %param.15) | copy-start | bytes 393220
  113.1 33.9 %copy-start.4 = (bf16[1024,64]{0,1:T(8,128)(2,1)S(1)}, bf16[1024,64]{0,1:T(8,128)(2,1)}, u32[]{:S(2)}) copy-start(bf16[1024,64]{0,1:T(8,128)(2,1)} %param.16) | copy-start | bytes 393220
  146.9 9.0 %copy-start.2 = (bf16[1024,256]{1,0:T(8,128)(2,1)S(1)}, bf16[1024,256]{1,0:T(8,128)(2,1)}, u32[]{:S(2)}) copy-start(bf16[1024,256]{1,0:T(8,128)(2,1)} %param.14) | copy-start | bytes 1572868
  146.9 9.0 %copy-start.5 = (f32[4]{0:T(128)S(1)}, f32[4]{0:T(128)}, u32[]{:S(2)}) copy-start(f32[4]{0:T(128)} %param.17) | copy-start | bytes 52
  146.9 98.7 %reduce-scatter.3.cloned.1.call-start = ((), (), s32[]{:S(2)}) async-start(), calls=%async_computation.4 | async-start | bytes 5242880 | tf_op jit(solution)/shard_map/reduce_scatter | solution.py:98
  147.0 5.4 %collective-permute-start = (bf16[128,128]{0,1:T(8,128)(2,1)S(1)}, bf16[128,128]{0,1:T(8,128)(2,1)S(1)}, u32[]{:S(2)}, u32[]{:S(2)}) collective-permute-start(bf16[128,128]{0,1:T(8,128)(2,1)S(1)} %get-tuple-element.131), channel_id=1, source_target_pairs={{0,4},{4,8},{8,12},{12,16},{16,20},{20,24},{24,28},{1,5},{5,9},{9,... | collective-permute-start | bytes 98312 | tf_op jit(solution)/shard_map/ppermute | solution.py:20
  150.3 5.6 %collective-permute-start.1 = (bf16[128,128]{0,1:T(8,128)(2,1)S(1)}, bf16[128,128]{0,1:T(8,128)(2,1)S(1)}, u32[]{:S(2)}, u32[]{:S(2)}) collective-permute-start(bf16[128,128]{0,1:T(8,128)(2,1)S(1)} %get-tuple-element.132), channel_id=1, source_target_pairs={{4,0},{8,4},{12,8},{16,12},{20,16},{24,20},{28,24},{5,1},{9,5},{13... | collective-permute-start | bytes 98312 | tf_op jit(solution)/shard_map/ppermute | solution.py:21
  159.7 2.7 %copy-start.1 = (f32[768,512,4]{1,0,2:T(8,128)}, f32[768,512,4]{1,0,2:T(8,128)S(1)}, u32[]{:S(2)}) copy-start(f32[768,512,4]{1,0,2:T(8,128)S(1)} %get-tuple-element.182) | copy-start | bytes 18874372 | tf_op jit(solution)/shard_map/while
  172.1 2.7 %copy-start.1 = (f32[768,512,4]{1,0,2:T(8,128)}, f32[768,512,4]{1,0,2:T(8,128)S(1)}, u32[]{:S(2)}) copy-start(f32[768,512,4]{1,0,2:T(8,128)S(1)} %get-tuple-element.182) | copy-start | bytes 18874372 | tf_op jit(solution)/shard_map/while
  181.0 22.4 %copy-start.6 = (f32[128,2]{0,1:T(2,128)S(1)}, f32[128,2]{0,1:T(2,128)}, u32[]{:S(2)}) copy-start(f32[128,2]{0,1:T(2,128)} %param.22) | copy-start | bytes 3076
  197.8 34.3 %all-to-all-start.1 = ((bf16[8,36,2048]{2,1,0:T(8,128)(2,1)}), bf16[8,36,2048]{2,1,0:T(8,128)(2,1)}, u32[]{:S(2)}, u32[]{:S(2)}) async-start(bf16[8,36,2048]{2,1,0:T(8,128)(2,1)} %reduce-scatter.5.cloned.1.call-done), calls=%async_computation.3 | async-start | bytes 2621440 | tf_op jit(solution)/shard_map/all_to_all | solution.py:142
Sparse Core Ops, SparseCore 0:
  53.7 39.8 all-gather.1
  147.0 50.7 reduce-scatter.4
  200.9 44.6 reduce-scatter.2
where the time goes:
time: 254 us; the launch traced here: 252 us
  waiting for transfers between devices  88.7 us (35%)
  matrix products  68 us (27%)
  blocking collectives  33.9 us (13%)
  local copies, waits for them, and re-layouts  22.4 us (9%)
  between operations  13.9 us (5%)
  other arithmetic  12.5 us (5%)
  starting transfers between devices  11 us (4%)
    all_gather x1, waiting for transfers between devices, body(): lax.all_gather(lax.all_to_all(outgoing, 'ep', split_axis=0, concat_axis=0...  40 us
    all_to_all x1, blocking collectives, body(): lax.all_to_all(outgoing, 'ep', split_axis=0, concat_axis=0, tiled=True)  33.9 us
    dot_general x1, matrix products, body(): jnp.einsum('scf,fd->scd', hidden, down_weight[0], preferred_element_type=...  33.8 us
    all_to_all x1, waiting for transfers between devices, body(): lax.all_to_all(summed.astype(jnp.bfloat16), 'ep', split_axis=0, concat_ax...  28.7 us
    dot_general x1, matrix products, expert_hidden(): jnp.einsum('scd,df->scf', arrived, up_weight[0], preferred_element_type=j...  19.5 us
    reduce_scatter x1, waiting for transfers between devices, body(): lax.psum_scatter(lax.optimization_barrier(rounded).astype(jnp.float32).as...  13.7 us
    dot_general x2, matrix products, one_block(): jnp.einsum('kgqs,skd->qkgd', weights.astype(jnp.bfloat16), value_block, p...  9.09 us
    all_to_all x1, starting transfers between devices, body(): lax.all_to_all(summed.astype(jnp.bfloat16), 'ep', split_axis=0, concat_ax...  5.48 us
  transfers between devices with their start and end apart: 6, of which 5 were waited for; matrix products, arithmetic and copies ran while one was open for 13% of the time, Pallas kernels for 0%

commit v1 on v0

v1 whole, which is shorter than its diff:
```python
import functools

import jax
import jax.numpy as jnp
from jax import lax
from jax.experimental import pallas as pl
from jax.experimental.pallas import tpu as pltpu
from jax.sharding import PartitionSpec as P

HEAD_DIM = 64
WINDOW = 128
EPS = 1e-06
BF = jnp.bfloat16
F32 = jnp.float32
MESH_ID = pl.DeviceIdType.MESH


def kernel(
    E,
    outgoing,
    q_in,
    kv_in,
    sink,
    wout_in,
    wg_in,
    wu_in,
    wd_in,
    mixed,
    results,
    arr,
    abuf,
    hid,
    wg,
    wu,
    wd,
    part,
    cx,
    cy,
    cz,
    cpre,
    fin,
    qb,
    kvb,
    wout,
    att,
    pp,
    px,
    py,
    pz,
    ppre,
    sem_load,
    a_send,
    a_recv,
    c_send,
    c_recv,
    x_send,
    x_recv,
    xc_send,
    xc_recv,
    h_send,
    h_recv,
    p_send,
    p_recv,
    g_send,
    g_recv,
    z_send,
    z_recv,
    r_send,
    r_recv,
):
    e = lax.axis_index("ep")
    t = lax.axis_index("tp")
    mate = t + 1 - 2 * lax.rem(t, 2)
    cross = lax.rem(t + 2, 4)
    far = lax.rem(mate + 2, 4)
    cap, width = outgoing.shape[1], outgoing.shape[2]
    rows = E * cap
    row_count = kv_in.shape[0]
    kv_width = kv_in.shape[1]
    heads = q_in.shape[0]
    ff = wg_in.shape[2]
    own_rows = row_count // 4

    def remote(src, dst, ssem, rsem, to_e, to_t):
        return pltpu.make_async_remote_copy(
            src_ref=src,
            dst_ref=dst,
            send_sem=ssem,
            recv_sem=rsem,
            device_id=(to_e, to_t),
            device_id_type=MESH_ID,
        )

    loads = [
        pltpu.make_async_copy(kv_in, kvb.at[pl.ds(WINDOW, row_count)], sem_load.at[0]),
        pltpu.make_async_copy(q_in, qb, sem_load.at[1]),
        pltpu.make_async_copy(outgoing.at[e], arr.at[t, e], sem_load.at[2]),
        pltpu.make_async_copy(wout_in, wout, sem_load.at[3]),
        pltpu.make_async_copy(wg_in.at[0], wg, sem_load.at[4]),
        pltpu.make_async_copy(wu_in.at[0], wu, sem_load.at[5]),
        pltpu.make_async_copy(wd_in.at[0], wd, sem_load.at[6]),
    ]
    for copy in loads:
        copy.start()

    barrier = pltpu.get_barrier_semaphore()
    for i in range(1, E):
        pl.semaphore_signal(barrier, inc=1, device_id=(lax.rem(e + i, E), t), device_id_type=MESH_ID)
    pl.semaphore_signal(barrier, inc=1, device_id=(e, mate), device_id_type=MESH_ID)
    pl.semaphore_signal(barrier, inc=1, device_id=(e, cross), device_id_type=MESH_ID)
    pl.semaphore_wait(barrier, E + 1)

    def to_core(i, src):
        s = lax.rem(e + E - i, E)
        return remote(src, arr.at[t, s], c_send.at[i], c_recv.at[i], e, mate)

    def to_cross(i, src):
        s = lax.rem(e + E - i, E)
        return remote(src, arr.at[t, s], x_send.at[i], x_recv.at[i], e, cross)

    def relay(i):
        s = lax.rem(e + E - i, E)
        return remote(arr.at[cross, s], arr.at[cross, s], xc_send.at[i], xc_recv.at[i], e, mate)

    def peer(i):
        d = lax.rem(e + i, E)
        return remote(outgoing.at[d], arr.at[t, e], a_send.at[i], a_recv.at[i], d, t)

    to_cross(0, outgoing.at[e]).start()
    halo_up = remote(
        kv_in.at[pl.ds(row_count - WINDOW, WINDOW)],
        kvb.at[pl.ds(0, WINDOW)],
        h_send.at[0],
        h_recv.at[0],
        lax.rem(e + 1, E),
        t,
    )
    halo_down = remote(
        kv_in.at[pl.ds(0, WINDOW)],
        kvb.at[pl.ds(WINDOW + row_count, WINDOW)],
        h_send.at[1],
        h_recv.at[1],
        lax.rem(e + E - 1, E),
        t,
    )
    halo_up.start()
    halo_down.start()
    for i in range(1, E):
        peer(i).start()
    to_core(0, outgoing.at[e]).start()

    def pump(i):
        peer(i).wait_recv()
        s = lax.rem(e + E - i, E)
        to_cross(i, arr.at[t, s]).start()
        to_core(i, arr.at[t, s]).start()

    def pump_cross(i):
        s = lax.rem(e + E - i, E)
        to_cross(i, arr.at[t, s]).wait_recv()
        relay(i).start()

    loads[0].wait()
    loads[1].wait()
    halo_up.wait_recv()
    halo_down.wait_recv()

    span = 3 * WINDOW
    blocks = row_count // WINDOW
    per_block = E // blocks
    last_block = blocks - 1

    def attention(b):
        start = pl.multiple_of(b * WINDOW, WINDOW)
        keys = kvb[pl.ds(start, span), 0:128]
        vals = kvb[pl.ds(start, span), 128:256]
        lane_v = lax.broadcasted_iota(jnp.int32, (span, 128), 1)
        one = jnp.ones((), BF)
        low_vals = jnp.where(lane_v < HEAD_DIM, vals, one)
        high_vals = jnp.where(lane_v >= HEAD_DIM, vals, one)
        row = lax.broadcasted_iota(jnp.int32, (WINDOW, span), 0)
        col = lax.broadcasted_iota(jnp.int32, (WINDOW, span), 1)
        first = jnp.where((e == 0) & (b == 0), WINDOW, 0)
        last = jnp.where((e == E - 1) & (b == last_block), 2 * WINDOW, span)
        inside = (col >= row) & (col <= row + 2 * WINDOW) & (col >= first) & (col < last)
        lane_o = lax.broadcasted_iota(jnp.int32, (WINDOW, 128), 1)
        outs = []
        for h in range(heads):
            q = qb[h, pl.ds(start, WINDOW), :]
            s = lax.dot_general(q, keys, (((1,), (1,)), ((), ())), preferred_element_type=F32)
            s = jnp.where(inside, s, -jnp.inf)
            sink_h = sink[h]
            peak = jnp.maximum(jnp.max(s, axis=1, keepdims=True), sink_h)
            w = jnp.exp(s - peak).astype(BF)
            rest = jnp.exp(sink_h - peak)
            o = jnp.dot(w, low_vals if h % 2 == 0 else high_vals, preferred_element_type=F32)
            total = (o[:, 127:128] if h % 2 == 0 else o[:, 0:1]) + rest
            outs.append(o / total)
        for pair in range(heads // 2):
            both = jnp.where(lane_o < HEAD_DIM, outs[2 * pair], outs[2 * pair + 1])
            att[pl.ds(start, WINDOW), 128 * pair : 128 * pair + 128] = both.astype(BF)

    def step(b, carry):
        attention(b)
        for k in range(per_block):
            i = b * per_block + k

            @pl.when(i > 0)
            def _():
                pump(i)

        return carry

    lax.fori_loop(0, blocks, step, 0)

    loads[3].wait()

    def project(o):
        a = att[pl.ds(pl.multiple_of(o * own_rows, own_rows), own_rows), :]

        def tile(j, carry):
            c = pl.ds(pl.multiple_of(j * 512, 512), 512)
            pp[o, :, c] = jnp.dot(a, wout[:, c], preferred_element_type=F32).astype(BF)
            return carry

        lax.fori_loop(0, width // 512, tile, 0)

    project(far)
    p_far = remote(pp.at[far], px, p_send.at[0], p_recv.at[0], e, mate)
    p_far.start()
    project(mate)
    p_mate = remote(pp.at[mate], py, p_send.at[1], p_recv.at[1], e, mate)
    p_mate.start()
    project(cross)
    project(t)
    p_far.wait_recv()
    ppre[...] = (pp[cross].astype(F32) + px[...].astype(F32)).astype(BF)

    half = E // 2
    for i in range(half):
        pump_cross(i)
    loads[2].wait()
    loads[4].wait()
    loads[5].wait()

    def expert(o, down_wait=None):
        abuf[...] = arr[o].reshape(rows, width)

        def up_tile(j, carry):
            c = pl.ds(pl.multiple_of(j * 256, 256), 256)
            a = abuf[...]
            g = jnp.dot(a, wg[:, c], preferred_element_type=F32)
            u = jnp.dot(a, wu[:, c], preferred_element_type=F32)
            hid[:, c] = (g / (1.0 + jnp.exp(-g)) * u).astype(BF)
            return carry

        lax.fori_loop(0, ff // 256, up_tile, 0)
        if down_wait is not None:
            down_wait()

        def down_tile(j, carry):
            c = pl.ds(pl.multiple_of(j * 256, 256), 256)
            r = jnp.dot(hid[...], wd[:, c], preferred_element_type=F32)
            for i in range(E):
                part[o, i, :, c] = r[i * cap : (i + 1) * cap].astype(BF)
            return carry

        lax.fori_loop(0, width // 256, down_tile, 0)

    expert(t, loads[6].wait)
    for i in range(half, E - E // 4):
        pump_cross(i)
    for i in range(E):
        to_core(i, arr.at[mate, 0]).wait_recv()
    expert(mate)
    g_mate = remote(part.at[mate], cy, g_send.at[1], g_recv.at[1], e, mate)
    g_mate.start()
    for i in range(E - E // 4, E):
        pump_cross(i)
    p_cross = remote(ppre, pz, p_send.at[2], p_recv.at[2], e, cross)
    p_cross.start()
    for i in range(E):
        relay(i).wait_recv()
    expert(far)
    g_far = remote(part.at[far], cx, g_send.at[0], g_recv.at[0], e, mate)
    g_far.start()
    expert(cross)
    g_far.wait_recv()

    def to_owner(i):
        s = lax.rem(e + i, E)
        return remote(cpre.at[s], cz.at[s], z_send.at[i], z_recv.at[i], e, cross)

    def give_back(i):
        s = lax.rem(e + i, E)
        return remote(fin.at[s], results.at[e], r_send.at[i], r_recv.at[i], s, t)

    order = list(range(1, E)) + [0]
    for i in order:
        s = lax.rem(e + i, E)
        cpre[s] = (part[cross, s].astype(F32) + cx[s].astype(F32)).astype(BF)
        to_owner(i).start()

    g_mate.wait_recv()
    p_mate.wait_recv()
    p_cross.wait_recv()
    mixed[...] = (pp[t].astype(F32) + py[...].astype(F32) + pz[...].astype(F32)).astype(BF)
    for i in order:
        s = lax.rem(e + i, E)
        to_owner(i).wait_recv()
        fin[s] = (part[t, s].astype(F32) + cy[s].astype(F32) + cz[s].astype(F32)).astype(BF)
        if i:
            give_back(i).start()
    keep = pltpu.make_async_copy(fin.at[e], results.at[e], sem_load.at[7])
    keep.start()
    for i in range(1, E):
        give_back(i).wait_recv()
    keep.wait()

    halo_up.wait_send()
    halo_down.wait_send()
    p_far.wait_send()
    p_mate.wait_send()
    p_cross.wait_send()
    g_far.wait_send()
    g_mate.wait_send()
    for i in range(E):
        to_core(i, arr.at[t, 0]).wait_send()
        to_cross(i, arr.at[t, 0]).wait_send()
        relay(i).wait_send()
        to_owner(i).wait_send()
        if i:
            peer(i).wait_send()
            give_back(i).wait_send()


def body(
    query_rows,
    key_rows,
    value_rows,
    sink_logit,
    out_weight,
    routed_rows,
    norm_gain,
    routing,
    route_weight,
    gate_weight,
    up_weight,
    down_weight,
):
    E = lax.axis_size("ep")
    row_count = query_rows.shape[0]
    heads = query_rows.shape[1] // HEAD_DIM
    ff = gate_weight.shape[2]
    q = (query_rows * jnp.asarray(HEAD_DIM**-0.5, BF)).reshape(row_count, heads, HEAD_DIM)
    q = jnp.pad(jnp.transpose(q, (1, 0, 2)), ((0, 0), (0, 0), (0, 128 - HEAD_DIM)))
    kv = jnp.concatenate([key_rows, jnp.zeros_like(key_rows), value_rows, value_rows], axis=1)

    token_count, width = routed_rows.shape
    top = routing.shape[1]
    cap = token_count * top * 9 // (8 * E)
    rows = E * cap
    values = routed_rows.astype(F32)
    normed = (
        values * lax.rsqrt(jnp.mean(values * values, axis=-1, keepdims=True) + EPS) * norm_gain
    ).astype(BF)
    chosen = routing.reshape(-1)
    count = chosen.shape[0]
    earlier = jnp.arange(count)[None, :] < jnp.arange(count)[:, None]
    slot = jnp.sum((earlier & (chosen[None, :] == chosen[:, None])).astype(jnp.int32), axis=1)
    target = (chosen * cap + slot).reshape(token_count, top)
    place = jnp.arange(rows, dtype=jnp.int32)
    hit = target[:, :, None] == place[None, None, :]
    spread = jnp.any(hit, axis=1).astype(BF)
    outgoing = lax.dot_general(
        spread, normed, (((0,), (0,)), ((), ())), preferred_element_type=F32
    ).astype(BF)
    outgoing = outgoing.reshape(E, cap, width)

    own = row_count // 4
    dma = pltpu.SemaphoreType.DMA
    block = (E, cap, width)
    any_spec = pl.BlockSpec(memory_space=pl.ANY)
    mixed, results = pl.pallas_call(
        functools.partial(kernel, E),
        out_shape=(
            jax.ShapeDtypeStruct((own, width), BF),
            jax.ShapeDtypeStruct(block, BF),
        ),
        in_specs=[
            any_spec,
            any_spec,
            any_spec,
            pl.BlockSpec(memory_space=pltpu.SMEM),
            any_spec,
            any_spec,
            any_spec,
            any_spec,
        ],
        out_specs=(pl.BlockSpec(memory_space=pltpu.VMEM), any_spec),
        scratch_shapes=[
            pltpu.VMEM((4,) + block, BF),
            pltpu.VMEM((rows, width), BF),
            pltpu.VMEM((rows, ff), BF),
            pltpu.VMEM((width, ff), BF),
            pltpu.VMEM((width, ff), BF),
            pltpu.VMEM((ff, width), BF),
            pltpu.VMEM((4,) + block, BF),
            pltpu.VMEM(block, BF),
            pltpu.VMEM(block, BF),
            pltpu.VMEM(block, BF),
            pltpu.VMEM(block, BF),
            pltpu.VMEM(block, BF),
            pltpu.VMEM(q.shape, BF),
            pltpu.VMEM((row_count + 2 * WINDOW, kv.shape[1]), BF),
            pltpu.VMEM(out_weight.shape, BF),
            pltpu.VMEM(query_rows.shape, BF),
            pltpu.VMEM((4, own, width), BF),
            pltpu.VMEM((own, width), BF),
            pltpu.VMEM((own, width), BF),
            pltpu.VMEM((own, width), BF),
            pltpu.VMEM((own, width), BF),
            dma((8,)),
            dma((E,)),
            dma((E,)),
            dma((E,)),
            dma((E,)),
            dma((E,)),
            dma((E,)),
            dma((E,)),
            dma((E,)),
            dma((2,)),
            dma((2,)),
            dma((3,)),
            dma((3,)),
            dma((2,)),
            dma((2,)),
            dma((E,)),
            dma((E,)),
            dma((E,)),
            dma((E,)),
        ],
        compiler_params=pltpu.CompilerParams(
            collective_id=0, has_side_effects=True, vmem_limit_bytes=64 * 1024 * 1024 - 131072
        ),
    )(outgoing, q, kv, sink_logit, out_weight, gate_weight, up_weight, down_weight)

    weight = jnp.sum(jnp.where(hit, route_weight[:, :, None], 0.0), axis=1)
    expert_mix = jnp.dot(
        weight,
        results.reshape(rows, width).astype(F32),
        precision=lax.Precision.HIGHEST,
        preferred_element_type=F32,
    ).astype(BF)
    return (mixed, expert_mix)


def solution(mesh):
    in_specs = (
        P("ep", "tp"),
        P("ep", "tp"),
        P("ep", "tp"),
        P("tp"),
        P("tp", None),
        P(("ep", "tp"), None),
        P(),
        P(("ep", "tp"), None),
        P(("ep", "tp"), None),
        P("ep", None, "tp"),
        P("ep", None, "tp"),
        P("ep", "tp", None),
    )
    out_specs = (P(("ep", "tp"), None), P(("ep", "tp"), None))
    return jax.shard_map(body, mesh=mesh, in_specs=in_specs, out_specs=out_specs, check_vma=False)
```

time: 254 us -> 138 us (0.54)
  Pallas kernels: 0 us -> 123 us
  waiting for transfers between devices: 88.7 us -> 0 us
  matrix products: 68 us -> 3.41 us
  blocking collectives: 33.9 us -> 0 us
  local copies, waits for them, and re-layouts: 22.4 us -> 7.02 us
  between operations: 13.9 us -> 0.78 us
  starting transfers between devices: 11 us -> 0 us
  other arithmetic: 12.5 us -> 3.26 us
    pallas_call x0 -> x1, Pallas kernels: none -> 123 us  [body(): pl.pallas_call(functools.partial(kernel, E), out_shape=(jax.ShapeDtypeStr...]
    dot_general x7 -> x2, matrix products: 68 us -> 3.41 us  [the longest x1 1.82 us: body(): jnp.dot(weight, results.reshape(rows, width).astype(F32), precision=lax.P...]
    all_gather x1 -> x0, waiting for transfers between devices: 40 us -> none  [body(): lax.all_gather(lax.all_to_all(outgoing, 'ep', split_axis=0, concat_axis=0...]
    all_to_all x1 -> x0, blocking collectives: 33.9 us -> none  [body(): lax.all_to_all(outgoing, 'ep', split_axis=0, concat_axis=0, tiled=True)]
    all_to_all x1 -> x0, waiting for transfers between devices: 28.7 us -> none  [body(): lax.all_to_all(summed.astype(jnp.bfloat16), 'ep', split_axis=0, concat_ax...]
    reduce_scatter x2 -> x0, waiting for transfers between devices: 16.6 us -> none  [the longest x1 13.7 us: body(): lax.psum_scatter(lax.optimization_barrier(rounded).astype(jnp.float32).as...]
    reduce_sum x4 -> x2, other arithmetic: 6.76 us -> 0.22 us  [the longest x1 0.19 us: body(): jnp.sum((earlier & (chosen[None, :] == chosen[:, None])).astype(jnp.int32...]
    all_to_all x1 -> x0, starting transfers between devices: 5.48 us -> none  [body(): lax.all_to_all(summed.astype(jnp.bfloat16), 'ep', split_axis=0, concat_ax...]
  transfers between devices with their start and end apart: 6 -> 0, of which waited for: 5 -> 0; matrix products, arithmetic and copies ran while one was open for 13% -> 0% of each run, Pallas kernels for 0% -> 0%
where the time goes in v1:
time: 138 us; the launch traced here: 137 us
  Pallas kernels  123 us (89%)
  local copies, waits for them, and re-layouts  7.02 us (5%)
  matrix products  3.41 us (2%)
  other arithmetic  3.26 us (2%)
    pallas_call x1, Pallas kernels, body(): pl.pallas_call(functools.partial(kernel, E), out_shape=(jax.ShapeDtypeStr...  123 us

profile of v1, /device:TPU:13, one launch (start us, length us, event | category | flops | bytes accessed | tf_op | source)
XLA Modules:
  0.0 137.4 jit_solution(5327439970336666246)
XLA Ops:
  0.6 0.8 copy.37
  1.4 0.1 eq.28
  1.6 0.2 convert_reduce_fusion
  1.7 0.1 reduce_sum.30
  1.9 0.1 copy.38
  2.0 0.7 multiply_add_fusion
  2.7 1.2 fusion
  3.9 1.6 %convolution_convert_fusion = bf16[288,2048]{1,0:T(8,128)(2,1)S(1)} fusion(pred[128,288]{0,1:T(8,128)(4,1)S(1)} %fusion.6, bf16[128,2048]{1,0:T(8,128)(2,1)} %param.17, f32[2048]{0:T(1024)} %param.18, f32[128]{0:T(128)S(1)} %add_rsqrt_fusion), kind=kOutput, calls=%fused_computation | convolution fusion | flops 152633344 | bytes 1749504 | tf_op jit(solution)/shard_map/dot_general | solution.py:375
  5.5 0.0 copy-start.1
  5.5 1.2 reshape.32.outgoing
  6.7 0.0 copy-done.1
  6.7 0.2 copy.39
  7.0 0.5 copy.40
  7.5 0.0 copy-start.2
  7.5 0.0 copy-start.3
  7.5 1.2 pad.4.q_in
  8.7 0.0 copy-done.2
  8.7 0.2 copy.41
  8.9 0.0 copy-done.3
  8.9 0.2 copy.42
  9.1 0.1 pad.6.clone
  9.1 1.0 pad_maximum_fusion.kv_in
  10.2 122.9 %shard_map.131 = (bf16[256,2048]{1,0:T(8,128)(2,1)}, bf16[8,36,2048]{2,1,0:T(8,128)(2,1)}) custom-call(bf16[8,36,2048]{2,1,0:T(8,128)(2,1)} %reshape.32.outgoing, bf16[4,1024,128]{2,1,0:T(8,128)(2,1)} %pad.4.q_in, bf16[1024,256]{1,0:T(8,128)(2,1)} %pad_maximum_fusion.kv_in, f32[4]{0:T(128)} %sink.1, bf16[256,2048]{1,0:T(8,128)(2,1)} %wout_in.1, ...), custom_call_target="tpu_custom_call" | custom-call | tf_op jit(solution)/shard_map/pallas_call | solution.py:384
  133.1 0.0 copy-start.4
  133.1 1.4 %reshape.34 = bf16[288,2048]{1,0:T(8,128)(2,1)S(1)} reshape(bf16[8,36,2048]{2,1,0:T(8,128)(2,1)} %get-tuple-element.5) | data formatting | bytes 2359296 | tf_op jit(solution)/shard_map/reshape | solution.py:451
  134.5 0.0 copy-done.4
  134.5 0.0 copy-start
  134.6 1.8 %convolution_convert_fusion.1 = bf16[128,2048]{1,0:T(8,128)(2,1)} fusion(f32[128,288]{0,1:T(8,128)S(1)} %select_reduce_fusion, bf16[288,2048]{1,0:T(8,128)(2,1)S(1)} %reshape.34), kind=kOutput, calls=%fused_computation.1 | convolution fusion | flops 906231808 | bytes 1851392 | tf_op jit(solution)/shard_map/dot_general | solution.py:449
  136.4 0.0 copy-done
  136.4 1.0 copy.45
  (5 shorter events, 0.1 us)
Async XLA Ops:
  5.5 1.2 copy-start.1
  7.5 1.2 copy-start.2
  7.5 1.4 copy-start.3
  133.1 1.4 %copy-start.4 = (f32[128,2]{0,1:T(2,128)S(1)}, f32[128,2]{0,1:T(2,128)}, u32[]{:S(2)}) copy-start(f32[128,2]{0,1:T(2,128)} %param.20) | copy-start | bytes 3076
  134.5 1.9 %copy-start = (bf16[256,2048]{1,0:T(8,128)(2,1)S(1)}, bf16[256,2048]{1,0:T(8,128)(2,1)}, u32[]{:S(2)}) copy-start(bf16[256,2048]{1,0:T(8,128)(2,1)} %get-tuple-element.8) | copy-start | bytes 3145732
